TPU v7x, 32 devices: a whole 2x2x4 slice. The times are simulated.
32 devices in a mesh: fs: 8 (over z, y), tp: 4 (over x, core).
Axes of the slice: x: 2, y: 2, z: 4, core: 2. Of those that a mesh axis runs over, the one named last changes fastest.
Arguments:
- inputs: bfloat16 [4096, 2112], P('fs', 'tp'), may hold values from -6 to 6
- w_conv_up: bfloat16 [2112, 2816], P('fs', 'tp'), may hold values from -0.125 to 0.125
- w_gate_up: bfloat16 [2112, 2816], P('fs', 'tp'), may hold values from -0.125 to 0.125
- w_down: bfloat16 [2816, 2112], P('tp', 'fs'), may hold values from -0.109375 to 0.109375
- taps: float32 [3, 2816], replicated, may hold values from -3 to 3
- conv_bias: float32 [2816], replicated, may hold values from -3 to 3
- cotangent: bfloat16 [4096, 2112], P('fs', 'tp'), may hold values from -6 to 6
Outputs:
- grad_inputs: bfloat16 [4096, 2112], P('fs', 'tp')
- grad_conv_up: float32 [2112, 2816], P('fs', 'tp')
- unit_norms: float32 [2816], P('tp')
- grad_taps: float32 [3, 2816], replicated
- grad_bias: float32 [2816], replicated
All inputs are finite; a program needn't handle non-finite values.
Results may differ from a plain program's by a relative error of at most 0.018.
Values may be sent and summed in bfloat16 or wider, within the bound.
A program may use at most 64 MiB of HBM per device.

v0:
```python
import math

import jax
import jax.numpy as jnp
from jax import lax
from jax.sharding import PartitionSpec as P

TAPS = 3


def shifted(block, axis, distance):
    devices = range(lax.axis_size(axis))
    route = [(i - distance, i) for i in devices if i - distance in devices]
    return lax.ppermute(block, axis, route)


def gelu_parts(value):
    normal_cdf = 0.5 * (1.0 + jax.scipy.special.erf(value / math.sqrt(2.0)))
    density = jnp.exp(-0.5 * value * value) / math.sqrt(2.0 * math.pi)
    return (value * normal_cdf, normal_cdf + value * density)


def per_device(inputs, w_conv_up, w_gate_up, w_down, taps, conv_bias, cotangent):
    span = TAPS - 1
    rows = inputs.shape[0]
    width = w_conv_up.shape[1]
    col_start = lax.axis_index("tp") * width
    taps_own = lax.dynamic_slice_in_dim(taps, col_start, width, 1)
    bias_own = lax.dynamic_slice_in_dim(conv_bias, col_start, width, 0)
    features, cot_full = (
        lax.all_gather(inputs, "tp", axis=1, tiled=True),
        lax.all_gather(cotangent, "tp", axis=1, tiled=True),
    )
    conv_weight, gate_weight = (
        lax.all_gather(w_conv_up, "fs", axis=0, tiled=True),
        lax.all_gather(w_gate_up, "fs", axis=0, tiled=True),
    )
    columns = cot_full
    d_hidden = lax.dot_general(
        columns,
        lax.all_gather(w_down, "fs", axis=1, tiled=True),
        (((1,), (1,)), ((), ())),
        preferred_element_type=jnp.float32,
    ).astype(jnp.bfloat16)
    up_a = jnp.dot(features, conv_weight, preferred_element_type=jnp.float32).astype(jnp.bfloat16)
    up_b = jnp.dot(features, gate_weight, preferred_element_type=jnp.float32).astype(jnp.bfloat16)
    earlier = shifted(up_a[rows - span :], "fs", 1)
    extended = jnp.concatenate([earlier, up_a], 0).astype(jnp.float32)
    conv_out = bias_own[None, :] + sum(
        (taps_own[i][None, :] * extended[i : i + rows] for i in range(TAPS))
    )
    gelu_value, gelu_slope = gelu_parts(conv_out)
    hidden_grad = d_hidden.astype(jnp.float32)
    d_conv = hidden_grad * up_b.astype(jnp.float32) * gelu_slope
    d_up_b = (hidden_grad * gelu_value).astype(jnp.bfloat16)
    later = shifted(d_conv[:span], "fs", -1)
    d_extended = jnp.concatenate([d_conv, later], 0)
    d_up_a = sum(
        (taps_own[i][None, :] * d_extended[span - i : span - i + rows] for i in range(TAPS))
    ).astype(jnp.bfloat16)
    tap_terms = [jnp.sum(d_conv * extended[i : i + rows], axis=0) for i in range(TAPS)]
    column_part = jnp.stack(tap_terms + [jnp.sum(d_conv, axis=0)], 0)
    contract = (((1,), (1,)), ((), ()))
    partial_sum = lax.dot_general(d_up_a, conv_weight, contract, preferred_element_type=jnp.float32)
    partial_sum = partial_sum + lax.dot_general(
        d_up_b, gate_weight, contract, preferred_element_type=jnp.float32
    )
    grad_inputs = lax.psum_scatter(
        partial_sum.astype(jnp.bfloat16), "tp", scatter_dimension=1, tiled=True
    )
    columns = features
    grad_conv_up = lax.psum_scatter(
        lax.dot_general(
            columns, d_up_a, (((0,), (0,)), ((), ())), preferred_element_type=jnp.float32
        ),
        "fs",
        scatter_dimension=0,
        tiled=True,
    )
    squares = jnp.sum(grad_conv_up * grad_conv_up, axis=0)
    placed = jnp.zeros((TAPS + 1, width * lax.axis_size("tp")), jnp.float32)
    placed = lax.dynamic_update_slice_in_dim(placed, column_part, col_start, 1)
    full_columns = lax.psum(placed, ("fs", "tp"))
    unit_norms = lax.psum(squares, "fs")
    return (grad_inputs, grad_conv_up, unit_norms, full_columns[:TAPS], full_columns[TAPS])


def solution(mesh):
    return jax.shard_map(
        per_device,
        mesh=mesh,
        in_specs=(
            P("fs", "tp"),
            P("fs", "tp"),
            P("fs", "tp"),
            P("tp", "fs"),
            P(),
            P(),
            P("fs", "tp"),
        ),
        out_specs=(P("fs", "tp"), P("fs", "tp"), P("tp"), P(), P()),
        check_vma=False,
    )
```

profile of v0, /device:TPU:0, one launch (start us, length us, event | category | flops | bytes accessed | tf_op | source)
XLA Modules:
  0.0 441.5 jit_solution(5598248172429005860)
XLA Ops:
  7.2 0.7 all-gather.10.cloned.1.call-update
  7.9 0.7 all-gather.14.cloned.1.call-update
  8.7 0.7 all-gather.6.cloned.1.call-update
  9.4 0.5 all-gather.8.cloned.1.call-update
  10.0 0.5 all-gather.12.cloned.1.call-update
  10.6 0.8 dynamic_slice.7
  11.4 0.9 dynamic-slice_reduce_fusion.2
  12.3 22.9 %all-gather.10.cloned.1.call-done = bf16[512,2112]{0,1:T(8,128)(2,1)} async-done(((bf16[512,528]{0,1:T(8,128)(2,1)}), bf16[512,2112]{0,1:T(8,128)(2,1)}) %all-gather.10.cloned.1.call-update) | async-done | bytes 2162704 | tf_op jit(solution)/shard_map/all_gather | solution.py:31
  35.2 63.3 %all-gather.14.cloned.1.call-done = bf16[2112,704]{1,0:T(8,128)(2,1)} async-done(((bf16[264,704]{1,0:T(8,128)(2,1)}), bf16[2112,704]{1,0:T(8,128)(2,1)}) %all-gather.14.cloned.1.call-update) | async-done | bytes 2973712 | tf_op jit(solution)/shard_map/all_gather | solution.py:35
  98.5 4.5 %convolution_convert_fusion = bf16[512,704]{0,1:T(8,128)(2,1)S(1)} fusion(bf16[512,2112]{0,1:T(8,128)(2,1)} %all-gather.10.cloned.1.call-done, bf16[2112,704]{1,0:T(8,128)(2,1)} %all-gather.14.cloned.1.call-done), kind=kOutput, calls=%fused_computation.26 | convolution fusion | flops 1522892800 | bytes 5857280 | tf_op jit(solution)/shard_map/dot_general | solution.py:45
  103.1 2.5 collective-permute-start
  105.5 16.1 %all-gather.6.cloned.1.call-done = bf16[512,2112]{0,1:T(8,128)(2,1)} async-done(((bf16[512,528]{0,1:T(8,128)(2,1)}), bf16[512,2112]{0,1:T(8,128)(2,1)}) %all-gather.6.cloned.1.call-update) | async-done | bytes 2162704 | tf_op jit(solution)/shard_map/all_gather | solution.py:32
  121.7 63.1 %all-gather.8.cloned.1.call-done = bf16[704,2112]{0,1:T(8,128)(2,1)} async-done(((bf16[704,264]{0,1:T(8,128)(2,1)}), bf16[704,2112]{0,1:T(8,128)(2,1)}) %all-gather.8.cloned.1.call-update) | async-done | bytes 2973712 | tf_op jit(solution)/shard_map/all_gather | solution.py:41
  184.8 4.5 %convolution_convert_fusion.2 = bf16[512,704]{0,1:T(8,128)(2,1)S(1)} fusion(bf16[512,2112]{0,1:T(8,128)(2,1)} %all-gather.6.cloned.1.call-done, bf16[704,2112]{0,1:T(8,128)(2,1)} %all-gather.8.cloned.1.call-done), kind=kOutput, calls=%fused_computation.28 | convolution fusion | flops 1522892800 | bytes 5857280 | tf_op jit(solution)/shard_map/dot_general | solution.py:39
  189.3 0.4 maximum_convert_fusion
  189.7 2.4 add_add_fusion
  192.1 54.5 %all-gather.12.cloned.1.call-done = bf16[2112,704]{1,0:T(8,128)(2,1)} async-done(((bf16[264,704]{1,0:T(8,128)(2,1)}), bf16[2112,704]{1,0:T(8,128)(2,1)}) %all-gather.12.cloned.1.call-update) | async-done | bytes 2973712 | tf_op jit(solution)/shard_map/all_gather | solution.py:36
  246.6 5.3 %fusion.6 = f32[512,704]{0,1:T(8,128)S(1)} fusion(bf16[512,704]{0,1:T(8,128)(2,1)S(1)} %convolution_convert_fusion.2, f32[512,704]{0,1:T(8,128)} %add_add_fusion, bf16[512,2112]{0,1:T(8,128)(2,1)} %all-gather.10.cloned.1.call-done, bf16[2112,704]{1,0:T(8,128)(2,1)} %all-gather.12.cloned.1.call-done), kind=kOutput, calls=%fused_computation.13 | convolution fusion | flops 1527218176 | bytes 8740864 | tf_op jit(solution)/shard_map/dot_general | solution.py:46
  251.9 1.4 collective-permute-start.1
  253.4 9.0 %collective-permute-done.1 = f32[2,704]{0,1:T(8,128)S(1)} collective-permute-done((f32[2,704]{0,1:T(8,128)S(1)}, f32[2,704]{0,1:T(8,128)S(1)}, u32[]{:S(2)}, u32[]{:S(2)}) %collective-permute-start.1) | collective-permute-done | bytes 5664 | tf_op jit(solution)/shard_map/ppermute | solution.py:14
  262.3 3.2 multiply_reduce_fusion.2
  265.6 4.5 %convolution_bitcast_fusion = f32[2112,704]{0,1:T(8,128)} fusion(bf16[512,704]{0,1:T(8,128)(2,1)S(1)} %get-tuple-element.22, bf16[512,2112]{0,1:T(8,128)(2,1)S(1)} %copy-done), kind=kOutput, calls=%fused_computation | convolution fusion | flops 1522532352 | bytes 8830976 | tf_op jit(solution)/shard_map/dot_general | solution.py:73
  270.1 7.2 %copy.14 = f32[2112,704]{1,0:T(8,128)} copy(f32[2112,704]{0,1:T(8,128)} %convolution_bitcast_fusion) | data formatting | bytes 11894784
  277.5 3.9 fusion.14
  281.5 3.3 fusion
  284.9 0.3 dynamic_update_slice.3
  285.2 44.6 %psum.15 = f32[4,2816]{1,0:T(4,128)S(1)} all-reduce(f32[4,2816]{1,0:T(4,128)S(1)} %dynamic_update_slice.3), channel_id=1, replica_groups=mesh['fs'=8,'tp'=4] {'fs','tp'}, use_global_device_ids=true, to_apply=%region_8.0 | all-reduce | flops 11264 | bytes 90112 | tf_op jit(solution)/shard_map/psum | solution.py:83
  329.9 0.6 slice_reduce_fusion
  330.5 70.1 %reduce-scatter.7.cloned.1.call-done = f32[264,704]{1,0:T(8,128)} async-done(((f32[2112,704]{1,0:T(8,128)}), f32[264,704]{1,0:T(8,128)}) %reduce-scatter.7.cloned.1.call-update) | async-done | bytes 743440
  400.6 1.5 copy.15
  402.3 20.3 %psum.14 = f32[704]{0:T(1024)} all-reduce(f32[704]{0:T(1024)S(1)} %multiply_reduce_fusion.3), channel_id=1, replica_groups=mesh['fs'=8,'tp'=4] {'fs'}, use_global_device_ids=true, to_apply=%region_3.0 | all-reduce | flops 704 | bytes 5632 | tf_op jit(solution)/shard_map/psum | solution.py:84
  422.6 12.0 %reduce-scatter.5.cloned.1.call-done = bf16[512,528]{0,1:T(8,128)(2,1)} async-done(((bf16[512,2112]{0,1:T(8,128)(2,1)}), bf16[512,528]{0,1:T(8,128)(2,1)}) %reduce-scatter.5.cloned.1.call-update) | async-done | bytes 540688 | tf_op jit(solution)/shard_map/reduce_scatter | solution.py:68
  (27 shorter events, 0.9 us)
Async XLA Ops:
  7.2 28.1 %all-gather.10.cloned.1.call-start = ((), (), s32[]{:S(2)}) async-start(), calls=%async_computation.4 | async-start | bytes 2703360 | tf_op jit(solution)/shard_map/all_gather | solution.py:31
  7.9 90.6 %all-gather.14.cloned.1.call-start = ((), (), s32[]{:S(2)}) async-start(), calls=%async_computation.6 | async-start | bytes 3649536 | tf_op jit(solution)/shard_map/all_gather | solution.py:35
  8.6 113.0 %all-gather.6.cloned.1.call-start = ((), (), s32[]{:S(2)}) async-start(), calls=%async_computation.2 | async-start | bytes 2703360 | tf_op jit(solution)/shard_map/all_gather | solution.py:32
  9.4 175.4 %all-gather.8.cloned.1.call-start = ((), (), s32[]{:S(2)}) async-start(), calls=%async_computation.3 | async-start | bytes 3649536 | tf_op jit(solution)/shard_map/all_gather | solution.py:41
  10.0 236.7 %all-gather.12.cloned.1.call-start = ((), (), s32[]{:S(2)}) async-start(), calls=%async_computation.5 | async-start | bytes 3649536 | tf_op jit(solution)/shard_map/all_gather | solution.py:36
  10.5 390.1 %reduce-scatter.7.cloned.1.call-start = ((), (), s32[]{:S(2)}) async-start(), calls=%async_computation.8 | async-start | bytes 7299072
  103.1 86.2 %collective-permute-start = (bf16[2,704]{0,1:T(8,128)(2,1)S(1)}, bf16[2,704]{0,1:T(8,128)(2,1)S(1)}, u32[]{:S(2)}, u32[]{:S(2)}) collective-permute-start(bf16[2,704]{0,1:T(8,128)(2,1)S(1)} %slice.54), channel_id=1, source_target_pairs={{0,4},{4,8},{8,12},{12,16},{16,20},{20,24},{24,28},{1,5},{5,9},{9,... | collective-permute-start | bytes 8456 | tf_op jit(solution)/shard_map/ppermute | solution.py:14
  251.9 13.6 %copy-start = (bf16[512,2112]{0,1:T(8,128)(2,1)S(1)}, bf16[512,2112]{0,1:T(8,128)(2,1)}, u32[]{:S(2)}) copy-start(bf16[512,2112]{0,1:T(8,128)(2,1)} %all-gather.10.cloned.1.call-done) | copy-start | bytes 6488068
  251.9 10.4 %collective-permute-start.1 = (f32[2,704]{0,1:T(8,128)S(1)}, f32[2,704]{0,1:T(8,128)S(1)}, u32[]{:S(2)}, u32[]{:S(2)}) collective-permute-start(f32[2,704]{0,1:T(8,128)S(1)} %slice.58), channel_id=1, source_target_pairs={{4,0},{8,4},{12,8},{16,12},{20,16},{24,20},{28,24},{5,1},{9,5},{13... | collective-permute-start | bytes 16904 | tf_op jit(solution)/shard_map/ppermute | solution.py:14
  277.3 4.2 copy-start.1
  277.3 157.3 %reduce-scatter.5.cloned.1.call-start = ((), (), s32[]{:S(2)}) async-start(), calls=%async_computation.7 | async-start | bytes 2703360 | tf_op jit(solution)/shard_map/reduce_scatter | solution.py:68
  277.5 3.9 copy-start.3
  329.9 72.4 %copy-start.2 = (f32[4,2816]{1,0:T(4,128)}, f32[4,2816]{1,0:T(4,128)S(1)}, u32[]{:S(2)}) copy-start(f32[4,2816]{1,0:T(4,128)S(1)} %psum.15) | copy-start | bytes 135172
Sparse Core Ops, SparseCore 0:
  9.5 25.6 all-gather.9
  37.4 61.0 all-gather.13
  100.1 21.5 all-gather.5
  123.7 61.0 all-gather.7
  186.8 59.7 all-gather.11
  277.4 123.1 reduce-scatter.6
  403.7 30.8 reduce-scatter.4
where the time goes:
time: 442 us; the launch traced here: 441 us
  waiting for transfers between devices  314 us (71%)
  blocking collectives  64.9 us (15%)
  matrix products  25.9 us (6%)
  between operations  14.3 us (3%)
  local copies, waits for them, and re-layouts  11.5 us (3%)
  other arithmetic  6.2 us (1%)
    unnamed x8, waiting for transfers between devices  73.2 us
    all_gather x1, waiting for transfers between devices, per_device(): lax.all_gather(w_conv_up, 'fs', axis=0, tiled=True)  63.3 us
    all_gather x1, waiting for transfers between devices, per_device(): lax.all_gather(w_down, 'fs', axis=1, tiled=True)  63.1 us
    all_gather x1, waiting for transfers between devices, per_device(): lax.all_gather(w_gate_up, 'fs', axis=0, tiled=True)  54.5 us
    psum x1, blocking collectives, per_device(): full_columns = lax.psum(placed, ('fs', 'tp'))  44.6 us
    all_gather x1, waiting for transfers between devices, per_device(): lax.all_gather(inputs, 'tp', axis=1, tiled=True)  22.9 us
    psum x1, blocking collectives, per_device(): unit_norms = lax.psum(squares, 'fs')  20.3 us
    all_gather x1, waiting for transfers between devices, per_device(): lax.all_gather(cotangent, 'tp', axis=1, tiled=True)  16.1 us
  transfers between devices with their start and end apart: 9, of which 8 were waited for; matrix products, arithmetic and copies ran while one was open for 5% of the time, Pallas kernels for 0%

commit v1 on v0

--- a/solution.py
+++ b/solution.py
@@ -1,11 +1,18 @@
+import functools
 import math
 
 import jax
 import jax.numpy as jnp
 from jax import lax
+from jax.experimental import pallas as pl
+from jax.experimental.pallas import tpu as pltpu
 from jax.sharding import PartitionSpec as P
 
 TAPS = 3
+LANES = 128
+MESH = pl.DeviceIdType.MESH
+VMEM = pl.BlockSpec(memory_space=pltpu.VMEM)
+ANY = pl.BlockSpec(memory_space=pl.ANY)
 
 
 def shifted(block, axis, distance):
@@ -20,7 +27,7 @@
     return (value * normal_cdf, normal_cdf + value * density)
 
 
-def per_device(inputs, w_conv_up, w_gate_up, w_down, taps, conv_bias, cotangent):
+def with_collectives(inputs, w_conv_up, w_gate_up, w_down, taps, conv_bias, cotangent):
     span = TAPS - 1
     rows = inputs.shape[0]
     width = w_conv_up.shape[1]
@@ -85,6 +92,351 @@
     return (grad_inputs, grad_conv_up, unit_norms, full_columns[:TAPS], full_columns[TAPS])
 
 
+def ring_member(place, n):
+    depth = n // 2
+    place = lax.rem(place + 2 * n, n)
+    side = place // depth
+    along = lax.rem(place, depth)
+    return (side * (depth - 1) + (1 - 2 * side) * along) * 2 + side
+
+
+def ring_place(index, n):
+    side = lax.rem(index, 2)
+    along = index // 2
+    return side * (n - 1 - 2 * along) + along
+
+
+def greet(peers):
+    barrier = pltpu.get_barrier_semaphore()
+    for peer in peers:
+        pl.semaphore_signal(barrier, inc=1, device_id=peer, device_id_type=MESH)
+    pl.semaphore_wait(barrier, len(peers))
+
+
+def gather_kernel(n, t, *refs):
+    weights, tokens = refs[:6], refs[6:8]
+    w_out, t_out = refs[8:14], refs[14:16]
+    send_sem, recv_sem, t_send, t_recv, own_sem = refs[16:]
+    me, mine = lax.axis_index("fs"), lax.axis_index("tp")
+    place = ring_place(me, n)
+    ways = (
+        {"fs": ring_member(place + 1, n)},
+        {"fs": ring_member(place - 1, n)},
+    )
+    peers = [{"tp": lax.rem(mine + k, t)} for k in range(1, t)]
+    greet(list(ways) + peers)
+    ring = []
+    for step in range(n - 1):
+        copies = []
+        for i in range(6):
+            way = i % 2
+            if step:
+                ring[step - 1][i].wait_recv()
+            owner = ring_member(place - step if way == 0 else place + step, n)
+            copy = pltpu.make_async_remote_copy(
+                src_ref=w_out[i].at[owner] if step else weights[i],
+                dst_ref=w_out[i].at[owner],
+                send_sem=send_sem.at[step, i],
+                recv_sem=recv_sem.at[step, i],
+                device_id=ways[way],
+                device_id_type=MESH,
+            )
+            copy.start()
+            copies.append(copy)
+        ring.append(copies)
+        if step == 0:
+            across = []
+            for i in range(2):
+                for k in range(1, t):
+                    copy = pltpu.make_async_remote_copy(
+                        src_ref=tokens[i],
+                        dst_ref=t_out[i].at[mine],
+                        send_sem=t_send.at[i, k - 1],
+                        recv_sem=t_recv.at[i, k - 1],
+                        device_id=peers[k - 1],
+                        device_id_type=MESH,
+                    )
+                    copy.start()
+                    across.append(copy)
+            own = [
+                pltpu.make_async_copy(weights[i], w_out[i].at[me], own_sem.at[i])
+                for i in range(6)
+            ] + [
+                pltpu.make_async_copy(tokens[i], t_out[i].at[mine], own_sem.at[6 + i])
+                for i in range(2)
+            ]
+            for copy in own:
+                copy.start()
+    for copy in ring[-1]:
+        copy.wait_recv()
+    for copy in across:
+        copy.wait_recv()
+    for copies in ring:
+        for copy in copies:
+            copy.wait_send()
+    for copy in across:
+        copy.wait_send()
+    for copy in own:
+        copy.wait()
+
+
+def gather_all(weights, tokens, n, t):
+    shape = jax.ShapeDtypeStruct
+    return pl.pallas_call(
+        functools.partial(gather_kernel, n, t),
+        out_shape=[shape((n,) + w.shape, w.dtype) for w in weights]
+        + [shape((t,) + x.shape, x.dtype) for x in tokens],
+        in_specs=[VMEM] * 8,
+        out_specs=[ANY] * 8,
+        scratch_shapes=[
+            pltpu.SemaphoreType.DMA((n - 1, 6)),
+            pltpu.SemaphoreType.DMA((n - 1, 6)),
+            pltpu.SemaphoreType.DMA((2, t - 1)),
+            pltpu.SemaphoreType.DMA((2, t - 1)),
+            pltpu.SemaphoreType.DMA((8,)),
+        ],
+        compiler_params=pltpu.CompilerParams(collective_id=0, has_side_effects=True),
+        name="gather_all",
+    )(*weights, *tokens)
+
+
+def reduce_kernel(n, t, *refs):
+    grads, partial, columns = refs[:2], refs[2], refs[3]
+    g_out, i_out, norm_out, col_out = refs[4:6], refs[6], refs[7], refs[8]
+    (sent, held, arrived, col_all, col_sum, norm_own, norm_all) = refs[9:16]
+    (send_sem, recv_sem, t_send, t_recv, c_send, c_recv, s_send, s_recv, n_send, n_recv) = refs[16:]
+    parts = grads[0].shape[1]
+    me, mine = lax.axis_index("fs"), lax.axis_index("tp")
+    place = ring_place(me, n)
+    ways = (
+        {"fs": ring_member(place + 1, n)},
+        {"fs": ring_member(place - 1, n)},
+    )
+    peers = [{"tp": lax.rem(mine + k, t)} for k in range(1, t)]
+    column = [{"fs": lax.rem(me + k, n)} for k in range(1, n)]
+    greet(column + peers)
+
+    def push(src, dst, send, recv, to):
+        copy = pltpu.make_async_remote_copy(
+            src_ref=src, dst_ref=dst, send_sem=send, recv_sem=recv,
+            device_id=to, device_id_type=MESH,
+        )
+        copy.start()
+        return copy
+
+    col_pushes = [
+        push(columns, col_all.at[me], c_send.at[k], c_recv.at[k], column[k])
+        for k in range(n - 1)
+    ]
+    across = [
+        push(
+            partial.at[lax.rem(mine + k, t)],
+            arrived.at[k - 1],
+            t_send.at[k - 1],
+            t_recv.at[k - 1],
+            peers[k - 1],
+        )
+        for k in range(1, t)
+    ]
+    ring = []
+    for step in range(n - 1):
+        copies = []
+        for c in range(parts):
+            for way in range(2):
+                ahead = place - 1 - step if way == 0 else place + 1 + step
+                value = grads[way][ring_member(ahead, n), c]
+                slot = c * 2 + way
+                if step:
+                    ring[step - 1][slot].wait_recv()
+                    value = value + held[step - 1, slot].astype(jnp.float32)
+                sent[step, slot] = value.astype(jnp.bfloat16)
+                copies.append(
+                    push(
+                        sent.at[step, slot],
+                        held.at[step, slot],
+                        send_sem.at[step, slot],
+                        recv_sem.at[step, slot],
+                        ways[way],
+                    )
+                )
+        ring.append(copies)
+        if step == 1:
+            for copy in col_pushes:
+                copy.wait_recv()
+            total = jnp.zeros(columns.shape, jnp.float32)
+            for k in range(n):
+                total = total + jnp.where(me == k, columns[...], col_all[k])
+            col_sum[...] = total
+            col_out[mine] = total
+            sum_pushes = [
+                push(col_sum, col_out.at[mine], s_send.at[k], s_recv.at[k], peers[k])
+                for k in range(t - 1)
+            ]
+    half = norm_own.shape[1] // 2
+    for way in range(2):
+        squares = jnp.zeros((1, half), jnp.float32)
+        for c in range(parts):
+            slot = c * 2 + way
+            ring[-1][slot].wait_recv()
+            value = grads[way][me, c] + held[n - 2, slot].astype(jnp.float32)
+            g_out[way][c] = value
+            squares = squares + jnp.sum(value * value, axis=0, keepdims=True)
+        norm_own[:, way * half : (way + 1) * half] = squares
+    norm_pushes = [
+        push(norm_own, norm_all.at[me], n_send.at[k], n_recv.at[k], column[k])
+        for k in range(n - 1)
+    ]
+    for copy in across:
+        copy.wait_recv()
+    rows = partial.shape[1]
+    piece = 16 if rows % 16 == 0 else 8
+
+    @pl.loop(0, rows // piece)
+    def _(r):
+        at = pl.ds(pl.multiple_of(r * piece, piece), piece)
+        total = partial[mine, at, :].astype(jnp.float32)
+        for k in range(t - 1):
+            total = total + arrived[k, at, :].astype(jnp.float32)
+        i_out[at, :] = total.astype(jnp.bfloat16)
+
+    for copy in norm_pushes:
+        copy.wait_recv()
+    total = jnp.zeros(norm_own.shape, jnp.float32)
+    for k in range(n):
+        total = total + jnp.where(me == k, norm_own[...], norm_all[k])
+    norm_out[...] = total
+    for copy in sum_pushes:
+        copy.wait_recv()
+    for copies in ring + [across, col_pushes, sum_pushes, norm_pushes]:
+        for copy in copies:
+            copy.wait_send()
+
+
+def reduce_all(grads, partial, columns, n, t):
+    shape = jax.ShapeDtypeStruct
+    parts, rows, half = grads[0].shape[1:]
+    dma = pltpu.SemaphoreType.DMA
+    blocks = pltpu.VMEM((n - 1, 2 * parts, rows, half), jnp.bfloat16)
+    return pl.pallas_call(
+        functools.partial(reduce_kernel, n, t),
+        out_shape=[shape((parts, rows, half), jnp.float32)] * 2
+        + [
+            shape(partial.shape[1:], jnp.bfloat16),
+            shape((1, 2 * half), jnp.float32),
+            shape((t,) + columns.shape, jnp.float32),
+        ],
+        in_specs=[VMEM] * 4,
+        out_specs=[VMEM] * 5,
+        scratch_shapes=[
+            blocks,
+            blocks,
+            pltpu.VMEM((t - 1,) + partial.shape[1:], jnp.bfloat16),
+            pltpu.VMEM((n,) + columns.shape, jnp.float32),
+            pltpu.VMEM(columns.shape, jnp.float32),
+            pltpu.VMEM((1, 2 * half), jnp.float32),
+            pltpu.VMEM((n, 1, 2 * half), jnp.float32),
+            dma((n - 1, 2 * parts)),
+            dma((n - 1, 2 * parts)),
+            dma((t - 1,)),
+            dma((t - 1,)),
+            dma((n - 1,)),
+            dma((n - 1,)),
+            dma((t - 1,)),
+            dma((t - 1,)),
+            dma((n - 1,)),
+            dma((n - 1,)),
+        ],
+        compiler_params=pltpu.CompilerParams(
+            collective_id=1, has_side_effects=True, vmem_limit_bytes=56 * 1024 * 1024
+        ),
+        name="reduce_all",
+    )(*grads, partial, columns)
+
+
+def split(array, half):
+    array = jnp.pad(array, ((0, 0), (0, 2 * half - array.shape[1])))
+    return [array[:, :half], array[:, half:]]
+
+
+def with_kernels(inputs, w_conv_up, w_gate_up, w_down, taps, conv_bias, cotangent):
+    n, t = lax.axis_size("fs"), lax.axis_size("tp")
+    span = TAPS - 1
+    rows = inputs.shape[0]
+    shard, width = w_conv_up.shape
+    half = -(-width // (2 * LANES)) * LANES
+    col_start = lax.axis_index("tp") * width
+    taps_own = jnp.pad(
+        lax.dynamic_slice_in_dim(taps, col_start, width, 1), ((0, 0), (0, 2 * half - width))
+    )
+    bias_own = jnp.pad(
+        lax.dynamic_slice_in_dim(conv_bias, col_start, width, 0), ((0, 2 * half - width),)
+    )
+    weights = [p for w in (w_down.T, w_conv_up, w_gate_up) for p in split(w, half)]
+    got = gather_all(weights, [inputs.T, cotangent.T], n, t)
+    down, conv, gate = [[g.reshape(n * shard, half) for g in got[i : i + 2]] for i in (0, 2, 4)]
+    features, cot_full = [g.reshape(-1, rows) for g in got[6:]]
+
+    def project(left, right):
+        dots = [
+            lax.dot_general(
+                left, r, (((0,), (0,)), ((), ())), preferred_element_type=jnp.float32
+            ).astype(jnp.bfloat16)
+            for r in right
+        ]
+        return jnp.concatenate(dots, 1)
+
+    up_a = project(features, conv)
+    earlier = shifted(up_a[rows - span :], "fs", 1)
+    d_hidden = project(cot_full, down)
+    up_b = project(features, gate)
+    extended = jnp.concatenate([earlier, up_a], 0).astype(jnp.float32)
+    conv_out = bias_own[None, :] + sum(
+        (taps_own[i][None, :] * extended[i : i + rows] for i in range(TAPS))
+    )
+    gelu_value, gelu_slope = gelu_parts(conv_out)
+    hidden_grad = d_hidden.astype(jnp.float32)
+    d_conv = hidden_grad * up_b.astype(jnp.float32) * gelu_slope
+    d_up_b = (hidden_grad * gelu_value).astype(jnp.bfloat16)
+    later = shifted(d_conv[:span], "fs", -1)
+    d_extended = jnp.concatenate([d_conv, later], 0)
+    d_up_a = sum(
+        (taps_own[i][None, :] * d_extended[span - i : span - i + rows] for i in range(TAPS))
+    ).astype(jnp.bfloat16)
+    tap_terms = [jnp.sum(d_conv * extended[i : i + rows], axis=0) for i in range(TAPS)]
+    column_part = jnp.stack(tap_terms + [jnp.sum(d_conv, axis=0)], 0)
+    partial_sum = 0.0
+    for weight, grad in ((conv, d_up_a), (gate, d_up_b)):
+        for h in range(2):
+            partial_sum = partial_sum + lax.dot_general(
+                weight[h],
+                grad[:, h * half : (h + 1) * half],
+                (((1,), (1,)), ((), ())),
+                preferred_element_type=jnp.float32,
+            )
+    partial = partial_sum.astype(jnp.bfloat16).reshape(t, -1, rows)
+    parts = next(p for p in (3, 4, 2, 1) if shard % (8 * p) == 0)
+    grads = [
+        jnp.dot(
+            features, d_up_a[:, h * half : (h + 1) * half], preferred_element_type=jnp.float32
+        ).reshape(n, parts, shard // parts, half)
+        for h in range(2)
+    ]
+    low, high, grad_inputs, norms, columns = reduce_all(grads, partial, column_part, n, t)
+    grad_conv_up = jnp.concatenate(
+        [low.reshape(shard, half), high.reshape(shard, half)[:, : width - half]], 1
+    )
+    full = columns[:, :, :width].transpose(1, 0, 2).reshape(TAPS + 1, t * width)
+    return (grad_inputs.T, grad_conv_up, norms[0, :width], full[:TAPS], full[TAPS])
+
+
+def per_device(inputs, w_conv_up, *rest):
+    n, t = lax.axis_size("fs"), lax.axis_size("tp")
+    aligned = w_conv_up.shape[0] % 8 == 0 and inputs.shape[1] % 8 == 0
+    small = n % 2 == 0 and 4 <= n <= 16 and 2 <= t <= 8
+    chosen = with_kernels if aligned and small else with_collectives
+    return chosen(inputs, w_conv_up, *rest)
+
+
 def solution(mesh):
     return jax.shard_map(
         per_device,

time: 442 us -> 210 us (0.48)
  waiting for transfers between devices: 314 us -> 9.99 us
  Pallas kernels: 0 us -> 146 us
  blocking collectives: 64.9 us -> 0 us
  between operations: 14.3 us -> 0.91 us
  other arithmetic: 6.2 us -> 10.9 us
    all_gather x5 -> x0, waiting for transfers between devices: 220 us -> none  [the longest x1 63.3 us: per_device(): lax.all_gather(w_conv_up, 'fs', axis=0, tiled=True)]
    pallas_call x0 -> x2, Pallas kernels: none -> 146 us  [the longest x1 99.6 us: gather_all(): pl.pallas_call(functools.partial(gather_kernel, n, t), out_shape=[shape((...]
    unnamed x8 -> x0, waiting for transfers between devices: 73.2 us -> none
    psum x2 -> x0, blocking collectives: 64.9 us -> none  [the longest x1 44.6 us: per_device(): full_columns = lax.psum(placed, ('fs', 'tp'))]
    reduce_scatter x1 -> x0, waiting for transfers between devices: 12 us -> none  [per_device(): lax.psum_scatter(partial_sum.astype(jnp.bfloat16), 'tp', scatter_dimensio...]
    unnamed x10 -> x31, local copies, waits for them, and re-layouts: 8.68 us -> 2.16 us
    slice x4 -> x8, local copies, waits for them, and re-layouts: 1.71 us -> 6.16 us  [the longest x2 3.96 us: split(): return [array[:, :half], array[:, half:]]]
    dot_general x6 -> x12, matrix products: 25.9 us -> 25.4 us  [the longest x6 12.8 us: project(): lax.dot_general(left, r, (((0,), (0,)), ((), ())), preferred_element_type...]
  transfers between devices with their start and end apart: 9 -> 2, of which waited for: 8 -> 1; matrix products, arithmetic and copies ran while one was open for 5% -> 5% of each run, Pallas kernels for 0% -> 0%
where the time goes in v1:
time: 210 us
  Pallas kernels  146 us (70%)
  matrix products  25.4 us (12%)
  other arithmetic  10.9 us (5%)
  local copies, waits for them, and re-layouts  10.7 us (5%)
  waiting for transfers between devices  9.99 us (5%)
  starting transfers between devices  5.71 us (3%)
    pallas_call x1, Pallas kernels, gather_all(): pl.pallas_call(functools.partial(gather_kernel, n, t), out_shape=[shape((...  99.6 us
    pallas_call x1, Pallas kernels, reduce_all(): pl.pallas_call(functools.partial(reduce_kernel, n, t), out_shape=[shape((...  46.4 us
    dot_general x6, matrix products, project(): lax.dot_general(left, r, (((0,), (0,)), ((), ())), preferred_element_type...  12.8 us
    ppermute x2, waiting for transfers between devices, shifted(): return lax.ppermute(block, axis, route)  9.99 us
    dot_general x4, matrix products, with_kernels(): lax.dot_general(weight[h], grad[:, h * half:(h + 1) * half], (((1,), (1,)...  6.55 us
    dot_general x2, matrix products, with_kernels(): jnp.dot(features, d_up_a[:, h * half:(h + 1) * half], preferred_element_t...  6.12 us
    ppermute x2, starting transfers between devices, shifted(): return lax.ppermute(block, axis, route)  5.71 us
  transfers between devices with their start and end apart: 2, of which 1 were waited for; matrix products, arithmetic and copies ran while one was open for 5% of the time, Pallas kernels for 0%

profile of v1, /device:TPU:0, one launch (start us, length us, event | category | flops | bytes accessed | tf_op | source)
XLA Modules:
  0.0 209.6 jit_solution(15733411812857549907)
XLA Ops:
  0.6 1.8 pad_slice_fusion.4
  2.5 2.1 %pad_slice_fusion.2 = (bf16[264,384]{1,0:T(8,128)(2,1)}, bf16[264,384]{1,0:T(8,128)(2,1)}, bf16[264,384]{1,0:T(8,128)(2,1)}, bf16[264,384]{1,0:T(8,128)(2,1)}) fusion(bf16[264,704]{1,0:T(8,128)(2,1)} %param.9, bf16[264,704]{1,0:T(8,128)(2,1)} %param.8), kind=kLoop, calls=%fused_computation.36 | loop fusion | bytes 2027520 | tf_op jit(solution)/shard_map/slice | solution.py:358
  4.6 99.6 %gather_all.1 = (bf16[8,264,384]{2,1,0:T(8,128)(2,1)}, bf16[8,264,384]{2,1,0:T(8,128)(2,1)}, bf16[8,264,384]{2,1,0:T(8,128)(2,1)}, bf16[8,264,384]{2,1,0:T(8,128...) custom-call(bf16[264,384]{1,0:T(8,128)(2,1)} %get-tuple-element.45.r, ...), custom_call_target="tpu_custom_call" | custom-call | tf_op jit(solution)/shard_map/gather_all/pallas_call | solution.py:185
  104.2 3.3 %convolution_convert_fusion.1 = bf16[512,384]{0,1:T(8,128)(2,1)S(1)} fusion(bf16[2112,512]{1,0:T(8,128)(2,1)} %bitcast.44, bf16[2112,384]{1,0:T(8,128)(2,1)} %bitcast.51), kind=kOutput, calls=%fused_computation.28 | convolution fusion | flops 830668800 | bytes 4177920 | tf_op jit(solution)/shard_map/dot_general | solution.py:381
  107.6 1.1 convolution_convert_fusion
  108.8 0.7 copy-done.9
  109.5 0.8 pad_maximum_fusion.3
  110.3 4.1 %collective-permute-start = (bf16[2,768]{0,1:T(8,128)(2,1)}, bf16[2,768]{0,1:T(8,128)(2,1)}, u32[]{:S(2)}, u32[]{:S(2)}) collective-permute-start(bf16[2,768]{0,1:T(8,128)(2,1)} %pad_maximum_fusion.3), channel_id=1, source_target_pairs={{0,4},{4,8},{8,12},{12,16},{16,20},{20,24},{24,28},{1,5},{5,9},{9,... | collective-permute-start | bytes 9224 | tf_op jit(solution)/shard_map/ppermute | solution.py:21
  114.4 3.3 %convolution_convert_fusion.4 = bf16[512,384]{0,1:T(8,128)(2,1)S(1)} fusion(bf16[2112,512]{1,0:T(8,128)(2,1)} %bitcast.66, bf16[2112,384]{1,0:T(8,128)(2,1)} %bitcast.69), kind=kOutput, calls=%fused_computation.31 | convolution fusion | flops 830668800 | bytes 4177920 | tf_op jit(solution)/shard_map/dot_general | solution.py:381
  117.8 1.1 convolution_convert_fusion.5
  119.2 1.9 convolution_convert_fusion.3
  121.1 1.9 convolution_convert_fusion.2
  123.1 0.8 dynamic_slice.7
  124.0 1.5 maximum_convert_fusion
  125.5 3.6 %multiply_reduce_fusion.2 = (f32[768]{0:T(1024)S(1)}, f32[768]{0:T(1024)S(1)}, f32[768]{0:T(1024)S(1)}, f32[768]{0:T(1024)S(1)}, f32[512,768]{0,1:T(8,128)S(1)}, /*index=5*/f32[512,768]{0,1:T(8,128)S(1)}) fusion(f32[514,768]{0,1:T(8,128)S(1)} %maximum_convert_fusion, bf16[512,384]{0,1:T(8,128)(2,1)S(1)} %copy-done.12, bf16[512,384]{0,1:T(8,128)(2,1)S(1)} %copy-done.11, ...), kind=kLoop, calls=%fused_computation.24 | loop fusion | flops 12186624 | bytes 9461760 | tf_op jit(solution)/shard_map/reduce_sum | solution.py:405
  129.7 1.6 collective-permute-start.1
  131.3 0.6 pad_maximum_fusion.4.refs_3_
  131.9 10.0 %collective-permute-done.1 = f32[2,768]{0,1:T(8,128)S(1)} collective-permute-done((f32[2,768]{0,1:T(8,128)S(1)}, f32[2,768]{0,1:T(8,128)S(1)}, u32[]{:S(2)}, u32[]{:S(2)}) %collective-permute-start.1) | collective-permute-done | bytes 6176 | tf_op jit(solution)/shard_map/ppermute | solution.py:21
  141.9 1.9 fusion.7
  143.8 1.3 fusion.21
  145.0 3.1 %fusion.15.refs_1_ = f32[8,3,88,384]{3,2,1,0:T(8,128)} fusion(bf16[8,3,88,512]{3,2,1,0:T(8,128)(2,1)S(1)} %bitcast.48, bf16[512,768]{0,1:T(8,128)(2,1)S(1)} %fusion.7), kind=kOutput, calls=%fused_computation.41 | convolution fusion | flops 830472192 | bytes 5799936 | tf_op jit(solution)/shard_map/dot_general | solution.py:419
  148.2 3.0 %fusion.17.refs_0_ = f32[8,3,88,384]{3,2,1,0:T(8,128)} fusion(bf16[8,3,88,512]{3,2,1,0:T(8,128)(2,1)S(1)} %bitcast.49, bf16[512,768]{0,1:T(8,128)(2,1)S(1)} %fusion.7), kind=kOutput, calls=%fused_computation.43 | convolution fusion | flops 830472192 | bytes 5799936 | tf_op jit(solution)/shard_map/dot_general | solution.py:419
  151.2 1.3 convolution_add_fusion.2
  152.6 1.3 convolution_add_fusion.1
  154.0 2.7 %fusion = bf16[2112,512]{1,0:T(8,128)(2,1)} fusion(f32[2112,512]{1,0:T(8,128)S(1)} %convolution_add_fusion.1, bf16[2112,384]{1,0:T(8,128)(2,1)S(1)} %bitcast.54, bf16[512,768]{0,1:T(8,128)(2,1)S(1)} %fusion.2), kind=kOutput, calls=%fused_computation.3 | convolution fusion | flops 832634880 | bytes 8503296 | tf_op jit(solution)/shard_map/dot_general | solution.py:410
  156.7 46.4 %reduce_all.1 = (f32[3,88,384]{2,1,0:T(8,128)}, f32[3,88,384]{2,1,0:T(8,128)}, bf16[528,512]{1,0:T(8,128)(2,1)}, f32[1,768]{1,0:T(1,128)}, f32[4,4,768]{2,1,0:T(4,128)}) custom-call(f32[8,3,88,384]{3,2,1,0:T(8,128)} %fusion.17.refs_0_, f32[8,3,88,384]{3,2,1,0:T(8,128)} %fusion.15.refs_1_, bf16[4,528,512]{2,1,0:T(8,128)(2,1)} %bitcast.50, ...), custom_call_target="tpu_custom_call" | custom-call | tf_op jit(solution)/shard_map/reduce_all/pallas_call | solution.py:320
  203.2 1.3 slice_reduce_fusion.1
  204.5 0.8 slice_bitcast_fusion
  205.4 0.7 squeeze.7
  206.1 0.7 slice.114
  206.8 2.1 pad_maximum_fusion.1
  208.8 0.8 copy.22
  (41 shorter events, 1.3 us)
Async XLA Ops:
  0.6 122.4 %copy-start = (f32[3,2816]{1,0:T(4,128)S(1)}, f32[3,2816]{1,0:T(4,128)}, u32[]{:S(2)}) copy-start(f32[3,2816]{1,0:T(4,128)} %param.11) | copy-start | bytes 101380
  104.2 3.4 %copy-start.1 = (bf16[4,528,512]{2,1,0:T(8,128)(2,1)S(1)}, bf16[4,528,512]{2,1,0:T(8,128)(2,1)}, u32[]{:S(2)}) copy-start(bf16[4,528,512]{2,1,0:T(8,128)(2,1)} %get-tuple-element.18) | copy-start | bytes 6488068
  104.2 3.4 %copy-start.7 = (bf16[8,264,384]{2,1,0:T(8,128)(2,1)S(1)}, bf16[8,264,384]{2,1,0:T(8,128)(2,1)}, u32[]{:S(2)}) copy-start(bf16[8,264,384]{2,1,0:T(8,128)(2,1)} %get-tuple-element.25) | copy-start | bytes 4866052
  108.7 0.7 copy-start.9
  110.3 13.7 %collective-permute-start = (bf16[2,768]{0,1:T(8,128)(2,1)}, bf16[2,768]{0,1:T(8,128)(2,1)}, u32[]{:S(2)}, u32[]{:S(2)}) collective-permute-start(bf16[2,768]{0,1:T(8,128)(2,1)} %pad_maximum_fusion.3), channel_id=1, source_target_pairs={{0,4},{4,8},{8,12},{12,16},{16,20},{20,24},{24,28},{1,5},{5,9},{9,... | collective-permute-start | bytes 9224 | tf_op jit(solution)/shard_map/ppermute | solution.py:21
  114.4 3.4 %copy-start.13 = (bf16[4,528,512]{2,1,0:T(8,128)(2,1)S(1)}, bf16[4,528,512]{2,1,0:T(8,128)(2,1)}, u32[]{:S(2)}) copy-start(bf16[4,528,512]{2,1,0:T(8,128)(2,1)} %get-tuple-element.19) | copy-start | bytes 6488068
  114.4 3.4 %copy-start.14 = (bf16[8,264,384]{2,1,0:T(8,128)(2,1)S(1)}, bf16[8,264,384]{2,1,0:T(8,128)(2,1)}, u32[]{:S(2)}) copy-start(bf16[8,264,384]{2,1,0:T(8,128)(2,1)} %get-tuple-element.20) | copy-start | bytes 4866052
  117.8 1.4 copy-start.5
  119.2 1.9 copy-start.3
  123.0 2.4 %copy-start.11 = (bf16[512,384]{0,1:T(8,128)(2,1)S(1)}, bf16[512,384]{0,1:T(8,128)(2,1)}, u32[]{:S(2)}) copy-start(bf16[512,384]{0,1:T(8,128)(2,1)} %convolution_convert_fusion.3) | copy-start | bytes 1179652
  123.0 2.4 %copy-start.12 = (bf16[512,384]{0,1:T(8,128)(2,1)S(1)}, bf16[512,384]{0,1:T(8,128)(2,1)}, u32[]{:S(2)}) copy-start(bf16[512,384]{0,1:T(8,128)(2,1)} %convolution_convert_fusion.2) | copy-start | bytes 1179652
  129.6 14.2 %copy-start.2 = (bf16[8,264,384]{2,1,0:T(8,128)(2,1)S(1)}, bf16[8,264,384]{2,1,0:T(8,128)(2,1)}, u32[]{:S(2)}) copy-start(bf16[8,264,384]{2,1,0:T(8,128)(2,1)} %get-tuple-element.24) | copy-start | bytes 4866052
  129.7 12.2 %collective-permute-start.1 = (f32[2,768]{0,1:T(8,128)S(1)}, f32[2,768]{0,1:T(8,128)S(1)}, u32[]{:S(2)}, u32[]{:S(2)}) collective-permute-start(f32[2,768]{0,1:T(8,128)S(1)} %slice.120), channel_id=1, source_target_pairs={{4,0},{8,4},{12,8},{16,12},{20,16},{24,20},{28,24},{5,1},{9,5},{13... | collective-permute-start | bytes 18440 | tf_op jit(solution)/shard_map/ppermute | solution.py:21
  148.2 3.0 %copy-start.8 = (bf16[8,264,384]{2,1,0:T(8,128)(2,1)S(1)}, bf16[8,264,384]{2,1,0:T(8,128)(2,1)}, u32[]{:S(2)}) copy-start(bf16[8,264,384]{2,1,0:T(8,128)(2,1)} %get-tuple-element.25) | copy-start | bytes 4866052
  151.2 1.4 copy-start.6
  152.6 1.4 copy-start.4
  203.2 5.7 %copy-start.10 = (bf16[528,512]{1,0:T(8,128)(2,1)S(1)}, bf16[528,512]{1,0:T(8,128)(2,1)}, u32[]{:S(2)}) copy-start(bf16[528,512]{1,0:T(8,128)(2,1)} %get-tuple-element.26) | copy-start | bytes 1622020

commit v2 on v1

--- a/solution.py
+++ b/solution.py
@@ -114,9 +114,11 @@
 
 
 def gather_kernel(n, t, *refs):
-    weights, tokens = refs[:6], refs[6:8]
-    w_out, t_out = refs[8:14], refs[14:16]
-    send_sem, recv_sem, t_send, t_recv, own_sem = refs[16:]
+    tokens, w_out, t_out = refs[3:5], refs[5:11], refs[11:13]
+    send_sem, recv_sem, t_send, t_recv, own_sem = refs[13:]
+    cut = w_out[0].shape[2]
+    spans = (pl.ds(0, cut), pl.ds(cut, w_out[1].shape[2]))
+    weights = [w.at[:, span] for w in refs[:3] for span in spans]
     me, mine = lax.axis_index("fs"), lax.axis_index("tp")
     place = ring_place(me, n)
     ways = (
@@ -180,13 +182,13 @@
         copy.wait()
 
 
-def gather_all(weights, tokens, n, t):
+def gather_all(weights, tokens, cuts, n, t):
     shape = jax.ShapeDtypeStruct
     return pl.pallas_call(
         functools.partial(gather_kernel, n, t),
-        out_shape=[shape((n,) + w.shape, w.dtype) for w in weights]
+        out_shape=[shape((n, w.shape[0], c), w.dtype) for w in weights for c in cuts]
         + [shape((t,) + x.shape, x.dtype) for x in tokens],
-        in_specs=[VMEM] * 8,
+        in_specs=[VMEM] * 5,
         out_specs=[ANY] * 8,
         scratch_shapes=[
             pltpu.SemaphoreType.DMA((n - 1, 6)),
@@ -202,9 +204,10 @@
 
 def reduce_kernel(n, t, *refs):
     grads, partial, columns = refs[:2], refs[2], refs[3]
-    g_out, i_out, norm_out, col_out = refs[4:6], refs[6], refs[7], refs[8]
-    (sent, held, arrived, col_all, col_sum, norm_own, norm_all) = refs[9:16]
-    (send_sem, recv_sem, t_send, t_recv, c_send, c_recv, s_send, s_recv, n_send, n_recv) = refs[16:]
+    g_out, i_out, norm_out, col_out = refs[4:8]
+    sent, held = refs[8:10], refs[10:12]
+    arrived, col_all, col_sum, norm_own, norm_all = refs[12:17]
+    (send_sem, recv_sem, t_send, t_recv, c_send, c_recv, s_send, s_recv, n_send, n_recv) = refs[17:]
     parts = grads[0].shape[1]
     me, mine = lax.axis_index("fs"), lax.axis_index("tp")
     place = ring_place(me, n)
@@ -248,12 +251,12 @@
                 slot = c * 2 + way
                 if step:
                     ring[step - 1][slot].wait_recv()
-                    value = value + held[step - 1, slot].astype(jnp.float32)
-                sent[step, slot] = value.astype(jnp.bfloat16)
+                    value = value + held[way][step - 1, c].astype(jnp.float32)
+                sent[way][step, c] = value.astype(jnp.bfloat16)
                 copies.append(
                     push(
-                        sent.at[step, slot],
-                        held.at[step, slot],
+                        sent[way].at[step, c],
+                        held[way].at[step, c],
                         send_sem.at[step, slot],
                         recv_sem.at[step, slot],
                         ways[way],
@@ -272,20 +275,6 @@
                 push(col_sum, col_out.at[mine], s_send.at[k], s_recv.at[k], peers[k])
                 for k in range(t - 1)
             ]
-    half = norm_own.shape[1] // 2
-    for way in range(2):
-        squares = jnp.zeros((1, half), jnp.float32)
-        for c in range(parts):
-            slot = c * 2 + way
-            ring[-1][slot].wait_recv()
-            value = grads[way][me, c] + held[n - 2, slot].astype(jnp.float32)
-            g_out[way][c] = value
-            squares = squares + jnp.sum(value * value, axis=0, keepdims=True)
-        norm_own[:, way * half : (way + 1) * half] = squares
-    norm_pushes = [
-        push(norm_own, norm_all.at[me], n_send.at[k], n_recv.at[k], column[k])
-        for k in range(n - 1)
-    ]
     for copy in across:
         copy.wait_recv()
     rows = partial.shape[1]
@@ -299,6 +288,23 @@
             total = total + arrived[k, at, :].astype(jnp.float32)
         i_out[at, :] = total.astype(jnp.bfloat16)
 
+    height = grads[0].shape[2]
+    start = 0
+    for way in range(2):
+        lanes = grads[way].shape[3]
+        squares = jnp.zeros((1, lanes), jnp.float32)
+        for c in range(parts):
+            slot = c * 2 + way
+            ring[-1][slot].wait_recv()
+            value = grads[way][me, c] + held[way][n - 2, c].astype(jnp.float32)
+            g_out[c * height : (c + 1) * height, start : start + lanes] = value
+            squares = squares + jnp.sum(value * value, axis=0, keepdims=True)
+        norm_own[:, start : start + lanes] = squares
+        start += lanes
+    norm_pushes = [
+        push(norm_own, norm_all.at[me], n_send.at[k], n_recv.at[k], column[k])
+        for k in range(n - 1)
+    ]
     for copy in norm_pushes:
         copy.wait_recv()
     total = jnp.zeros(norm_own.shape, jnp.float32)
@@ -314,27 +320,28 @@
 
 def reduce_all(grads, partial, columns, n, t):
     shape = jax.ShapeDtypeStruct
-    parts, rows, half = grads[0].shape[1:]
+    parts, rows = grads[0].shape[1:3]
+    width = sum(g.shape[3] for g in grads)
     dma = pltpu.SemaphoreType.DMA
-    blocks = pltpu.VMEM((n - 1, 2 * parts, rows, half), jnp.bfloat16)
+    blocks = [pltpu.VMEM((n - 1,) + g.shape[1:], jnp.bfloat16) for g in grads]
     return pl.pallas_call(
         functools.partial(reduce_kernel, n, t),
-        out_shape=[shape((parts, rows, half), jnp.float32)] * 2
-        + [
+        out_shape=[
+            shape((parts * rows, width), jnp.float32),
             shape(partial.shape[1:], jnp.bfloat16),
-            shape((1, 2 * half), jnp.float32),
+            shape((1, width), jnp.float32),
             shape((t,) + columns.shape, jnp.float32),
         ],
         in_specs=[VMEM] * 4,
-        out_specs=[VMEM] * 5,
+        out_specs=[VMEM] * 4,
         scratch_shapes=[
-            blocks,
-            blocks,
+            *blocks,
+            *blocks,
             pltpu.VMEM((t - 1,) + partial.shape[1:], jnp.bfloat16),
             pltpu.VMEM((n,) + columns.shape, jnp.float32),
             pltpu.VMEM(columns.shape, jnp.float32),
-            pltpu.VMEM((1, 2 * half), jnp.float32),
-            pltpu.VMEM((n, 1, 2 * half), jnp.float32),
+            pltpu.VMEM((1, width), jnp.float32),
+            pltpu.VMEM((n, 1, width), jnp.float32),
             dma((n - 1, 2 * parts)),
             dma((n - 1, 2 * parts)),
             dma((t - 1,)),
@@ -353,9 +360,31 @@
     )(*grads, partial, columns)
 
 
-def split(array, half):
-    array = jnp.pad(array, ((0, 0), (0, 2 * half - array.shape[1])))
-    return [array[:, :half], array[:, half:]]
+def halo_kernel(n, block, out, send_sem, recv_sem):
+    me = lax.axis_index("fs")
+    before, after = {"fs": lax.rem(me + n - 1, n)}, {"fs": lax.rem(me + 1, n)}
+    greet([before, after])
+    copy = pltpu.make_async_remote_copy(
+        src_ref=block, dst_ref=out, send_sem=send_sem, recv_sem=recv_sem,
+        device_id=before, device_id_type=MESH,
+    )
+    copy.start()
+    copy.wait()
+
+
+def from_next(block, n):
+    got = pl.pallas_call(
+        functools.partial(halo_kernel, n),
+        out_shape=jax.ShapeDtypeStruct(block.shape, block.dtype),
+        in_specs=[VMEM],
+        out_specs=VMEM,
+        scratch_shapes=[pltpu.SemaphoreType.DMA, pltpu.SemaphoreType.DMA],
+        compiler_params=pltpu.CompilerParams(
+            collective_id=2, has_side_effects=True, vmem_limit_bytes=1024 * 1024
+        ),
+        name="from_next",
+    )(block)
+    return jnp.where(lax.axis_index("fs") == n - 1, 0.0, got)
 
 
 def with_kernels(inputs, w_conv_up, w_gate_up, w_down, taps, conv_bias, cotangent):
@@ -365,15 +394,12 @@
     shard, width = w_conv_up.shape
     half = -(-width // (2 * LANES)) * LANES
     col_start = lax.axis_index("tp") * width
-    taps_own = jnp.pad(
-        lax.dynamic_slice_in_dim(taps, col_start, width, 1), ((0, 0), (0, 2 * half - width))
-    )
-    bias_own = jnp.pad(
-        lax.dynamic_slice_in_dim(conv_bias, col_start, width, 0), ((0, 2 * half - width),)
-    )
-    weights = [p for w in (w_down.T, w_conv_up, w_gate_up) for p in split(w, half)]
-    got = gather_all(weights, [inputs.T, cotangent.T], n, t)
-    down, conv, gate = [[g.reshape(n * shard, half) for g in got[i : i + 2]] for i in (0, 2, 4)]
+    cuts = (half, width - half)
+    starts = ((0, half), (half, width))
+    taps_own = lax.dynamic_slice_in_dim(taps, col_start, width, 1)
+    bias_own = lax.dynamic_slice_in_dim(conv_bias, col_start, width, 0)
+    got = gather_all([w_down.T, w_conv_up, w_gate_up], [inputs.T, cotangent.T], cuts, n, t)
+    down, conv, gate = [[g.reshape(n * shard, -1) for g in got[i : i + 2]] for i in (0, 2, 4)]
     features, cot_full = [g.reshape(-1, rows) for g in got[6:]]
 
     def project(left, right):
@@ -397,7 +423,7 @@
     hidden_grad = d_hidden.astype(jnp.float32)
     d_conv = hidden_grad * up_b.astype(jnp.float32) * gelu_slope
     d_up_b = (hidden_grad * gelu_value).astype(jnp.bfloat16)
-    later = shifted(d_conv[:span], "fs", -1)
+    later = from_next(d_conv[:8], n)[:span]
     d_extended = jnp.concatenate([d_conv, later], 0)
     d_up_a = sum(
         (taps_own[i][None, :] * d_extended[span - i : span - i + rows] for i in range(TAPS))
@@ -409,7 +435,7 @@
         for h in range(2):
             partial_sum = partial_sum + lax.dot_general(
                 weight[h],
-                grad[:, h * half : (h + 1) * half],
+                grad[:, slice(*starts[h])],
                 (((1,), (1,)), ((), ())),
                 preferred_element_type=jnp.float32,
             )
@@ -417,16 +443,13 @@
     parts = next(p for p in (3, 4, 2, 1) if shard % (8 * p) == 0)
     grads = [
         jnp.dot(
-            features, d_up_a[:, h * half : (h + 1) * half], preferred_element_type=jnp.float32
-        ).reshape(n, parts, shard // parts, half)
+            features, d_up_a[:, slice(*starts[h])], preferred_element_type=jnp.float32
+        ).reshape(n, parts, shard // parts, cuts[h])
         for h in range(2)
     ]
-    low, high, grad_inputs, norms, columns = reduce_all(grads, partial, column_part, n, t)
-    grad_conv_up = jnp.concatenate(
-        [low.reshape(shard, half), high.reshape(shard, half)[:, : width - half]], 1
-    )
-    full = columns[:, :, :width].transpose(1, 0, 2).reshape(TAPS + 1, t * width)
-    return (grad_inputs.T, grad_conv_up, norms[0, :width], full[:TAPS], full[TAPS])
+    grad_conv_up, grad_inputs, norms, columns = reduce_all(grads, partial, column_part, n, t)
+    full = columns.transpose(1, 0, 2).reshape(TAPS + 1, t * width)
+    return (grad_inputs.T, grad_conv_up, norms[0], full[:TAPS], full[TAPS])
 
 
 def per_device(inputs, w_conv_up, *rest):

time: 210 us -> 199 us (0.948)
  waiting for transfers between devices: 9.99 us -> 0.01 us
  other arithmetic: 10.9 us -> 6.61 us
  Pallas kernels: 146 us -> 150 us
  starting transfers between devices: 5.71 us -> 3.42 us
    ppermute x2 -> x1, waiting for transfers between devices: 9.99 us -> 0.01 us  [shifted(): return lax.ppermute(block, axis, route)]
    pallas_call x0 -> x1, Pallas kernels: none -> 4.88 us  [from_next(): pl.pallas_call(functools.partial(halo_kernel, n), out_shape=jax.ShapeDtyp...]
    slice x7 -> x4, local copies, waits for them, and re-layouts: 6.13 us -> 2.45 us  [the longest x3 2.45 us: with_kernels(): return (grad_inputs.T, grad_conv_up, norms[0], full[:TAPS], full[TAPS])]
    convert_element_type x0 -> x3, local copies, waits for them, and re-layouts: none -> 3.29 us  [project(): dots = [lax.dot_general(left, r, (((0,), (0,)), ((), ())), preferred_elem...]
    ppermute x2 -> x1, starting transfers between devices: 5.71 us -> 3.42 us  [shifted(): return lax.ppermute(block, axis, route)]
  transfers between devices with their start and end apart: 2 -> 1, of which waited for: 1 -> 0; matrix products, arithmetic and copies ran while one was open for 5% -> 6% of each run, Pallas kernels for 0% -> 0%
where the time goes in v2:
time: 199 us; the launch traced here: 198 us
  Pallas kernels  150 us (75%)
  matrix products  25.8 us (13%)
  local copies, waits for them, and re-layouts  11.2 us (6%)
  other arithmetic  6.61 us (3%)
  starting transfers between devices  3.42 us (2%)
    pallas_call x1, Pallas kernels, gather_all(): pl.pallas_call(functools.partial(gather_kernel, n, t), out_shape=[shape((...  99.5 us
    pallas_call x1, Pallas kernels, reduce_all(): pl.pallas_call(functools.partial(reduce_kernel, n, t), out_shape=[shape((...  46 us
    dot_general x6, matrix products, project(): lax.dot_general(left, r, (((0,), (0,)), ((), ())), preferred_element_type...  13.1 us
    dot_general x4, matrix products, with_kernels(): lax.dot_general(weight[h], grad[:, slice(*starts[h])], (((1,), (1,)), (()...  6.62 us
    dot_general x2, matrix products, with_kernels(): jnp.dot(features, d_up_a[:, slice(*starts[h])], preferred_element_type=jn...  6.04 us
    pallas_call x1, Pallas kernels, from_next(): pl.pallas_call(functools.partial(halo_kernel, n), out_shape=jax.ShapeDtyp...  4.88 us
  transfers between devices with their start and end apart: 1, of which 0 were waited for; matrix products, arithmetic and copies ran while one was open for 6% of the time, Pallas kernels for 0%

profile of v2, /device:TPU:0, one launch (start us, length us, event | category | flops | bytes accessed | tf_op | source)
XLA Modules:
  0.0 198.3 jit_solution(5762420604894979779)
XLA Ops:
  0.6 99.5 %gather_all.1 = (bf16[8,264,384]{2,1,0:T(8,128)(2,1)}, bf16[8,264,320]{2,1,0:T(8,128)(2,1)}, bf16[8,264,384]{2,1,0:T(8,128)(2,1)}, bf16[8,264,320]{2,1,0:T(8,128...) custom-call(bf16[264,704]{1,0:T(8,128)(2,1)} %bitcast.63, ...), custom_call_target="tpu_custom_call" | custom-call | tf_op jit(solution)/shard_map/gather_all/pallas_call | solution.py:187
  100.1 3.2 %convolution_convert_fusion.3 = bf16[512,320]{0,1:T(8,128)(2,1)S(1)} fusion(bf16[2112,512]{1,0:T(8,128)(2,1)} %bitcast.42, bf16[2112,320]{1,0:T(8,128)(2,1)} %bitcast.58), kind=kOutput, calls=%fused_computation.30 | convolution fusion | flops 692224000 | bytes 3842048 | tf_op jit(solution)/shard_map/dot_general | solution.py:407
  103.3 0.2 copy.32
  103.6 3.0 %convolution_convert_fusion = bf16[512,384]{1,0:T(8,128)(2,1)S(1)} fusion(bf16[2112,512]{1,0:T(8,128)(2,1)S(1)} %bitcast.43, bf16[2112,384]{1,0:T(8,128)(2,1)} %bitcast.48), kind=kOutput, calls=%fused_computation.27 | convolution fusion | flops 830668800 | bytes 4177920 | tf_op jit(solution)/shard_map/dot_general | solution.py:407
  106.6 3.4 %collective-permute-start = (bf16[2,704]{1,0:T(2,128)(2,1)S(1)}, bf16[2,704]{1,0:T(2,128)(2,1)S(1)}, u32[]{:S(2)}, u32[]{:S(2)}) collective-permute-start(bf16[2,704]{1,0:T(2,128)(2,1)S(1)} %pad_maximum_fusion.3), channel_id=1, source_target_pairs={{0,4},{4,8},{8,12},{12,16},{16,20},{20,24},{24,28},{1,5},{5,9},{9,... | collective-permute-start | bytes 8456 | tf_op jit(solution)/shard_map/ppermute | solution.py:21
  110.1 1.7 convolution_convert_fusion.5
  111.8 1.4 convolution_convert_fusion.2
  113.2 2.2 %convolution_convert_fusion.1 = bf16[512,384]{1,0:T(8,128)(2,1)} fusion(bf16[2112,512]{1,0:T(8,128)(2,1)S(1)} %bitcast.44, bf16[2112,384]{1,0:T(8,128)(2,1)S(1)} %bitcast.51), kind=kOutput, calls=%fused_computation.28 | convolution fusion | flops 830668800 | bytes 4177920 | tf_op jit(solution)/shard_map/dot_general | solution.py:407
  115.4 1.7 convolution_convert_fusion.4
  117.1 1.2 copy.28
  118.3 1.9 copy.30
  120.2 0.8 dynamic_slice.7
  121.0 0.9 dynamic-slice_reduce_fusion.2
  121.9 1.2 maximum_convert_fusion
  123.1 2.0 %multiply_reduce_fusion.2 = (f32[704]{0:T(1024)S(1)}, f32[704]{0:T(1024)S(1)}, f32[704]{0:T(1024)S(1)}, f32[704]{0:T(1024)S(1)}, f32[512,704]{1,0:T(8,128)S(1)}, /*index=5*/f32[512,704]{1,0:T(8,128)S(1)}) fusion(f32[514,704]{1,0:T(8,128)S(1)} %maximum_convert_fusion, bf16[512,320]{1,0:T(8,128)(2,1)S(1)} %copy-done.11, bf16[512,384]{1,0:T(8,128)(2,1)S(1)} %copy-done.10, ...), kind=kLoop, calls=%fused_computation.24 | loop fusion | flops 11171072 | bytes 8673280 | tf_op jit(solution)/shard_map/reduce_sum | solution.py:431
  125.1 4.9 %from_next.1 = f32[8,704]{1,0:T(8,128)S(1)} custom-call(f32[8,704]{1,0:T(8,128)S(1)} %slice.84.block), custom_call_target="tpu_custom_call" | custom-call | tf_op jit(solution)/shard_map/from_next/pallas_call | solution.py:376
  130.0 1.5 fusion.5
  131.6 1.3 fusion.21
  132.9 3.1 %fusion.17.refs_1_ = f32[8,3,88,320]{3,2,1,0:T(8,128)} fusion(bf16[8,3,88,512]{3,2,1,0:T(8,128)(2,1)S(1)} %bitcast.46, bf16[512,704]{1,0:T(8,128)(2,1)S(1)} %get-tuple-element.38), kind=kOutput, calls=%fused_computation.39 | convolution fusion | flops 692060160 | bytes 5259264 | tf_op jit(solution)/shard_map/dot_general | solution.py:445
  136.0 3.0 %fusion.15.refs_0_ = f32[8,3,88,384]{3,2,1,0:T(8,128)} fusion(bf16[8,3,88,512]{3,2,1,0:T(8,128)(2,1)S(1)} %bitcast.47, bf16[512,704]{1,0:T(8,128)(2,1)S(1)} %get-tuple-element.38), kind=kOutput, calls=%fused_computation.37 | convolution fusion | flops 830472192 | bytes 5799936 | tf_op jit(solution)/shard_map/dot_general | solution.py:445
  139.0 1.3 convolution_add_fusion.2
  140.4 1.3 convolution_add_fusion.1
  141.8 2.7 %fusion = bf16[2112,512]{1,0:T(8,128)(2,1)} fusion(f32[2112,512]{1,0:T(8,128)S(1)} %convolution_add_fusion.1, bf16[2112,320]{1,0:T(8,128)(2,1)S(1)} %bitcast.56, bf16[512,704]{1,0:T(8,128)(2,1)S(1)} %get-tuple-element.39), kind=kOutput, calls=%fused_computation.3 | convolution fusion | flops 694222848 | bytes 8503296 | tf_op jit(solution)/shard_map/dot_general | solution.py:436
  144.5 0.6 pad_maximum_fusion.2.refs_3_
  145.1 46.0 %reduce_all.1 = (f32[264,704]{1,0:T(8,128)}, bf16[528,512]{1,0:T(8,128)(2,1)}, f32[1,704]{1,0:T(1,128)}, f32[4,4,704]{2,1,0:T(4,128)}) custom-call(f32[8,3,88,384]{3,2,1,0:T(8,128)} %fusion.15.refs_0_, f32[8,3,88,320]{3,2,1,0:T(8,128)} %fusion.17.refs_1_, bf16[4,528,512]{2,1,0:T(8,128)(2,1)} %bitcast.50, f32[4,704]{1,0:T(4,128)} %pad_maximum_fusion.2.refs_3_), custom_call_target="tpu_custom_call" | custom-call | tf_op jit(solution)/shard_map/reduce_all/pallas_call | solution.py:327
  191.1 0.9 slice_reduce_fusion
  192.1 0.7 squeeze.7
  192.7 0.8 copy.34
  193.6 0.7 slice.79
  194.3 1.3 reduce.3
  195.6 1.9 copy.43
  197.4 0.9 copy.44
  (36 shorter events, 0.3 us)
Async XLA Ops:
  100.1 3.4 %copy-start = (bf16[4,528,512]{2,1,0:T(8,128)(2,1)S(1)}, bf16[4,528,512]{2,1,0:T(8,128)(2,1)}, u32[]{:S(2)}) copy-start(bf16[4,528,512]{2,1,0:T(8,128)(2,1)} %get-tuple-element.17) | copy-start | bytes 6488068
  103.5 3.0 %copy-start.4 = (bf16[512,320]{1,0:T(8,128)(2,1)}, bf16[512,320]{1,0:T(8,128)(2,1)S(1)}, u32[]{:S(2)}) copy-start(bf16[512,320]{1,0:T(8,128)(2,1)S(1)} %copy.32) | copy-start | bytes 983044
  103.6 6.5 %copy-start.5 = (bf16[4,528,512]{2,1,0:T(8,128)(2,1)S(1)}, bf16[4,528,512]{2,1,0:T(8,128)(2,1)}, u32[]{:S(2)}) copy-start(bf16[4,528,512]{2,1,0:T(8,128)(2,1)} %get-tuple-element.18) | copy-start | bytes 6488068
  103.6 6.5 %copy-start.13 = (bf16[8,264,320]{2,1,0:T(8,128)(2,1)S(1)}, bf16[8,264,320]{2,1,0:T(8,128)(2,1)}, u32[]{:S(2)}) copy-start(bf16[8,264,320]{2,1,0:T(8,128)(2,1)} %get-tuple-element.20) | copy-start | bytes 4055044
  106.6 15.3 %collective-permute-start = (bf16[2,704]{1,0:T(2,128)(2,1)S(1)}, bf16[2,704]{1,0:T(2,128)(2,1)S(1)}, u32[]{:S(2)}, u32[]{:S(2)}) collective-permute-start(bf16[2,704]{1,0:T(2,128)(2,1)S(1)} %pad_maximum_fusion.3), channel_id=1, source_target_pairs={{0,4},{4,8},{8,12},{12,16},{16,20},{20,24},{24,28},{1,5},{5,9},{9,... | collective-permute-start | bytes 8456 | tf_op jit(solution)/shard_map/ppermute | solution.py:21
  110.1 1.7 copy-start.8
  111.8 1.4 copy-start.2
  113.2 2.2 %copy-start.6 = (bf16[8,264,320]{2,1,0:T(8,128)(2,1)S(1)}, bf16[8,264,320]{2,1,0:T(8,128)(2,1)}, u32[]{:S(2)}) copy-start(bf16[8,264,320]{2,1,0:T(8,128)(2,1)} %get-tuple-element.22) | copy-start | bytes 4055044
  120.1 3.0 %copy-start.10 = (bf16[512,384]{1,0:T(8,128)(2,1)S(1)}, bf16[512,384]{1,0:T(8,128)(2,1)}, u32[]{:S(2)}) copy-start(bf16[512,384]{1,0:T(8,128)(2,1)} %convolution_convert_fusion.1) | copy-start | bytes 1179652
  120.1 3.0 %copy-start.11 = (bf16[512,320]{1,0:T(8,128)(2,1)S(1)}, bf16[512,320]{1,0:T(8,128)(2,1)}, u32[]{:S(2)}) copy-start(bf16[512,320]{1,0:T(8,128)(2,1)} %copy.30) | copy-start | bytes 983044
  130.0 1.6 copy-start.1
  136.0 3.0 %copy-start.9 = (bf16[8,264,320]{2,1,0:T(8,128)(2,1)S(1)}, bf16[8,264,320]{2,1,0:T(8,128)(2,1)}, u32[]{:S(2)}) copy-start(bf16[8,264,320]{2,1,0:T(8,128)(2,1)} %get-tuple-element.24) | copy-start | bytes 4055044
  139.0 1.4 copy-start.3
  140.4 1.4 copy-start.7
  191.1 6.3 %copy-start.12 = (f32[264,704]{1,0:T(8,128)S(1)}, f32[264,704]{1,0:T(8,128)}, u32[]{:S(2)}) copy-start(f32[264,704]{1,0:T(8,128)} %get-tuple-element.46) | copy-start | bytes 2230276

commit v3 on v2

--- a/solution.py
+++ b/solution.py
@@ -114,10 +114,13 @@
 
 
 def gather_kernel(n, t, *refs):
-    tokens, w_out, t_out = refs[3:5], refs[5:11], refs[11:13]
-    send_sem, recv_sem, t_send, t_recv, own_sem = refs[13:]
-    cut = w_out[0].shape[2]
-    spans = (pl.ds(0, cut), pl.ds(cut, w_out[1].shape[2]))
+    tokens, grown, projected = refs[3:5], refs[5:10], refs[10:13]
+    w_out = refs[13:15] + grown[:4]
+    t_out = (grown[4], refs[15])
+    totals = refs[16:22]
+    send_sem, recv_sem, t_send, t_recv = refs[22:]
+    cut, rest = w_out[0].shape[2], w_out[1].shape[2]
+    spans = (pl.ds(0, cut), pl.ds(cut, rest))
     weights = [w.at[:, span] for w in refs[:3] for span in spans]
     me, mine = lax.axis_index("fs"), lax.axis_index("tp")
     place = ring_place(me, n)
@@ -126,78 +129,106 @@
         {"fs": ring_member(place - 1, n)},
     )
     peers = [{"tp": lax.rem(mine + k, t)} for k in range(1, t)]
+    blocks = tokens[0].shape[0]
+    held = pl.ds(mine * blocks, blocks)
     greet(list(ways) + peers)
+
+    def push(src, dst, send, recv, to):
+        copy = pltpu.make_async_remote_copy(
+            src_ref=src, dst_ref=dst, send_sem=send, recv_sem=recv,
+            device_id=to, device_id_type=MESH,
+        )
+        copy.start()
+        return copy
+
+    def owner_of(i, step):
+        return ring_member(place - step if i % 2 == 0 else place + step, n)
+
+    def multiply(step, i):
+        owner = owner_of(i, step)
+        product = lax.dot_general(
+            t_out[1 if i < 2 else 0][owner],
+            w_out[i][owner],
+            (((0,), (0,)), ((), ())),
+            preferred_element_type=jnp.float32,
+        )
+        totals[i][...] = totals[i][...] + product if step else product
+
+    first = min(3, n - 2)
+    waiting = [(step, i) for step in range(n) for i in range(6)]
     ring = []
     for step in range(n - 1):
         copies = []
         for i in range(6):
-            way = i % 2
             if step:
                 ring[step - 1][i].wait_recv()
-            owner = ring_member(place - step if way == 0 else place + step, n)
-            copy = pltpu.make_async_remote_copy(
-                src_ref=w_out[i].at[owner] if step else weights[i],
-                dst_ref=w_out[i].at[owner],
-                send_sem=send_sem.at[step, i],
-                recv_sem=recv_sem.at[step, i],
-                device_id=ways[way],
-                device_id_type=MESH,
+            owner = owner_of(i, step)
+            copies.append(
+                push(
+                    w_out[i].at[owner] if step else weights[i],
+                    w_out[i].at[owner],
+                    send_sem.at[step, i],
+                    recv_sem.at[step, i],
+                    ways[i % 2],
+                )
             )
-            copy.start()
-            copies.append(copy)
+            if step == first and i == 0:
+                for copy in across:
+                    copy.wait_recv()
+            if step >= first:
+                for _ in range(2):
+                    if waiting[0] <= (step, i):
+                        multiply(*waiting.pop(0))
         ring.append(copies)
         if step == 0:
-            across = []
+            across = [
+                push(
+                    tokens[i],
+                    t_out[i].at[held],
+                    t_send.at[i, k - 1],
+                    t_recv.at[i, k - 1],
+                    peers[k - 1],
+                )
+                for i in range(2)
+                for k in range(1, t)
+            ]
+            for i in range(6):
+                w_out[i][me] = refs[i // 2][:, (i % 2) * cut : cut + (i % 2) * rest]
             for i in range(2):
-                for k in range(1, t):
-                    copy = pltpu.make_async_remote_copy(
-                        src_ref=tokens[i],
-                        dst_ref=t_out[i].at[mine],
-                        send_sem=t_send.at[i, k - 1],
-                        recv_sem=t_recv.at[i, k - 1],
-                        device_id=peers[k - 1],
-                        device_id_type=MESH,
-                    )
-                    copy.start()
-                    across.append(copy)
-            own = [
-                pltpu.make_async_copy(weights[i], w_out[i].at[me], own_sem.at[i])
-                for i in range(6)
-            ] + [
-                pltpu.make_async_copy(tokens[i], t_out[i].at[mine], own_sem.at[6 + i])
-                for i in range(2)
-            ]
-            for copy in own:
-                copy.start()
-    for copy in ring[-1]:
-        copy.wait_recv()
-    for copy in across:
-        copy.wait_recv()
-    for copies in ring:
+                t_out[i][held] = tokens[i][...]
+    for step, i in waiting:
+        if step == n - 1:
+            ring[-1][i].wait_recv()
+        multiply(step, i)
+    for i in range(6):
+        projected[i // 2][:, (i % 2) * cut : cut + (i % 2) * rest] = totals[i][...].astype(
+            jnp.bfloat16
+        )
+    for copies in ring + [across]:
         for copy in copies:
             copy.wait_send()
-    for copy in across:
-        copy.wait_send()
-    for copy in own:
-        copy.wait()
 
 
 def gather_all(weights, tokens, cuts, n, t):
-    shape = jax.ShapeDtypeStruct
+    shape, kind = jax.ShapeDtypeStruct, jnp.bfloat16
+    shard, width = weights[0].shape
+    rows = tokens[0].shape[1]
+    tokens = [x.reshape(-1, shard, rows) for x in tokens]
+    dma = pltpu.SemaphoreType.DMA
     return pl.pallas_call(
         functools.partial(gather_kernel, n, t),
-        out_shape=[shape((n, w.shape[0], c), w.dtype) for w in weights for c in cuts]
-        + [shape((t,) + x.shape, x.dtype) for x in tokens],
+        out_shape=[shape((n, shard, c), kind) for _ in range(2) for c in cuts]
+        + [shape((n, shard, rows), kind)]
+        + [shape((rows, width), kind)] * 3,
         in_specs=[VMEM] * 5,
-        out_specs=[ANY] * 8,
-        scratch_shapes=[
-            pltpu.SemaphoreType.DMA((n - 1, 6)),
-            pltpu.SemaphoreType.DMA((n - 1, 6)),
-            pltpu.SemaphoreType.DMA((2, t - 1)),
-            pltpu.SemaphoreType.DMA((2, t - 1)),
-            pltpu.SemaphoreType.DMA((8,)),
-        ],
-        compiler_params=pltpu.CompilerParams(collective_id=0, has_side_effects=True),
+        out_specs=[VMEM] * 8,
+        scratch_shapes=[pltpu.VMEM((n, shard, c), kind) for c in cuts]
+        + [pltpu.VMEM((n, shard, rows), kind)]
+        + [pltpu.VMEM((rows, c), jnp.float32) for _ in range(3) for c in cuts]
+        + [dma((n - 1, 6)), dma((n - 1, 6)), dma((2, t - 1)), dma((2, t - 1))],
+        compiler_params=pltpu.CompilerParams(
+            collective_id=0, has_side_effects=True, vmem_limit_bytes=56 * 1024 * 1024
+        ),
         name="gather_all",
     )(*weights, *tokens)
 
@@ -399,22 +430,10 @@
     taps_own = lax.dynamic_slice_in_dim(taps, col_start, width, 1)
     bias_own = lax.dynamic_slice_in_dim(conv_bias, col_start, width, 0)
     got = gather_all([w_down.T, w_conv_up, w_gate_up], [inputs.T, cotangent.T], cuts, n, t)
-    down, conv, gate = [[g.reshape(n * shard, -1) for g in got[i : i + 2]] for i in (0, 2, 4)]
-    features, cot_full = [g.reshape(-1, rows) for g in got[6:]]
-
-    def project(left, right):
-        dots = [
-            lax.dot_general(
-                left, r, (((0,), (0,)), ((), ())), preferred_element_type=jnp.float32
-            ).astype(jnp.bfloat16)
-            for r in right
-        ]
-        return jnp.concatenate(dots, 1)
-
-    up_a = project(features, conv)
+    conv, gate = [[g.reshape(n * shard, -1) for g in got[i : i + 2]] for i in (0, 2)]
+    features = got[4].reshape(-1, rows)
+    d_hidden, up_a, up_b = got[5:]
     earlier = shifted(up_a[rows - span :], "fs", 1)
-    d_hidden = project(cot_full, down)
-    up_b = project(features, gate)
     extended = jnp.concatenate([earlier, up_a], 0).astype(jnp.float32)
     conv_out = bias_own[None, :] + sum(
         (taps_own[i][None, :] * extended[i : i + rows] for i in range(TAPS))
@@ -454,7 +473,7 @@
 
 def per_device(inputs, w_conv_up, *rest):
     n, t = lax.axis_size("fs"), lax.axis_size("tp")
-    aligned = w_conv_up.shape[0] % 8 == 0 and inputs.shape[1] % 8 == 0
+    aligned = w_conv_up.shape[0] % 8 == 0 and inputs.shape[1] % w_conv_up.shape[0] == 0
     small = n % 2 == 0 and 4 <= n <= 16 and 2 <= t <= 8
     chosen = with_kernels if aligned and small else with_collectives
     return chosen(inputs, w_conv_up, *rest)

time: 199 us -> 188 us (0.945)
  matrix products: 25.8 us -> 12.7 us
  Pallas kernels: 150 us -> 155 us
  local copies, waits for them, and re-layouts: 11.2 us -> 9.17 us
    dot_general x6 -> x0, matrix products: 13.1 us -> none  [project(): lax.dot_general(left, r, (((0,), (0,)), ((), ())), preferred_element_type...]
    pallas_call x1, Pallas kernels: 46 us -> 51.5 us  [reduce_all(): pl.pallas_call(functools.partial(reduce_kernel, n, t), out_shape=[shape((...]
    convert_element_type x3 -> x0, local copies, waits for them, and re-layouts: 3.29 us -> none  [project(): dots = [lax.dot_general(left, r, (((0,), (0,)), ((), ())), preferred_elem...]
  transfers between devices with their start and end apart: 1 -> 1, of which waited for: 0 -> 0; matrix products, arithmetic and copies ran while one was open for 6% -> 1% of each run, Pallas kernels for 0% -> 0%
where the time goes in v3:
time: 188 us; the launch traced here: 187 us
  Pallas kernels  155 us (82%)
  matrix products  12.7 us (7%)
  local copies, waits for them, and re-layouts  9.17 us (5%)
  other arithmetic  6.1 us (3%)
  starting transfers between devices  3.46 us (2%)
    pallas_call x1, Pallas kernels, gather_all(): pl.pallas_call(functools.partial(gather_kernel, n, t), out_shape=[shape((...  98.2 us
    pallas_call x1, Pallas kernels, reduce_all(): pl.pallas_call(functools.partial(reduce_kernel, n, t), out_shape=[shape((...  51.5 us
    dot_general x4, matrix products, with_kernels(): lax.dot_general(weight[h], grad[:, slice(*starts[h])], (((1,), (1,)), (()...  6.7 us
    dot_general x2, matrix products, with_kernels(): jnp.dot(features, d_up_a[:, slice(*starts[h])], preferred_element_type=jn...  5.98 us
    pallas_call x1, Pallas kernels, from_next(): pl.pallas_call(functools.partial(halo_kernel, n), out_shape=jax.ShapeDtyp...  5.44 us
  transfers between devices with their start and end apart: 1, of which 0 were waited for; matrix products, arithmetic and copies ran while one was open for 1% of the time, Pallas kernels for 0%

profile of v3, /device:TPU:0, one launch (start us, length us, event | category | flops | bytes accessed | tf_op | source)
XLA Modules:
  0.0 187.3 jit_solution(11072292679934279530)
XLA Ops:
  0.6 98.2 %gather_all.1 = (bf16[8,264,384]{2,1,0:T(8,128)(2,1)}, bf16[8,264,320]{2,1,0:T(8,128)(2,1)}, bf16[8,264,384]{2,1,0:T(8,128)(2,1)}, bf16[8,264,320]{2,1,0:T(8,128...) custom-call(bf16[264,704]{1,0:T(8,128)(2,1)} %bitcast.40, ...), custom_call_target="tpu_custom_call" | custom-call | tf_op jit(solution)/shard_map/gather_all/pallas_call | solution.py:218
  98.8 0.0 copy-start.2
  98.8 0.0 copy-start.7
  98.8 0.8 slice.64
  99.7 3.5 %collective-permute-start = (bf16[2,704]{1,0:T(2,128)(2,1)S(1)}, bf16[2,704]{1,0:T(2,128)(2,1)S(1)}, u32[]{:S(2)}, u32[]{:S(2)}) collective-permute-start(bf16[2,704]{1,0:T(2,128)(2,1)S(1)} %slice.64), channel_id=1, source_target_pairs={{0,4},{4,8},{8,12},{12,16},{16,20},{20,24},{24,28},{1,5},{5,9},{9,... | collective-permute-start | bytes 8456 | tf_op jit(solution)/shard_map/ppermute | solution.py:21
  103.1 0.8 dynamic_slice.7
  103.9 0.9 dynamic-slice_reduce_fusion.2
  104.8 0.0 collective-permute-done
  104.8 1.3 maximum_convert_fusion
  106.1 0.0 copy-done.2
  106.2 1.8 multiply_reduce_fusion.2
  108.0 5.4 %from_next.1 = f32[8,704]{1,0:T(8,128)S(1)} custom-call(f32[8,704]{1,0:T(8,128)S(1)} %slice.84.block), custom_call_target="tpu_custom_call" | custom-call | tf_op jit(solution)/shard_map/from_next/pallas_call | solution.py:407
  113.4 1.1 fusion.5
  114.6 0.5 copy-done
  115.0 3.0 %fusion.17.refs_1_ = f32[8,3,88,320]{3,2,1,0:T(8,128)} fusion(bf16[8,3,88,512]{3,2,1,0:T(8,128)(2,1)S(1)} %bitcast.30, bf16[512,704]{1,0:T(8,128)(2,1)S(1)} %get-tuple-element.38), kind=kOutput, calls=%fused_computation.32 | convolution fusion | flops 692060160 | bytes 5259264 | tf_op jit(solution)/shard_map/dot_general | solution.py:464
  118.1 3.0 %fusion.15.refs_0_ = f32[8,3,88,384]{3,2,1,0:T(8,128)} fusion(bf16[8,3,88,512]{3,2,1,0:T(8,128)(2,1)S(1)} %bitcast.31, bf16[512,704]{1,0:T(8,128)(2,1)S(1)} %get-tuple-element.38), kind=kOutput, calls=%fused_computation.30 | convolution fusion | flops 830472192 | bytes 5799936 | tf_op jit(solution)/shard_map/dot_general | solution.py:464
  121.1 1.3 fusion.21
  122.4 0.1 copy-done.5
  122.5 1.4 convolution_add_fusion.2
  123.9 0.0 copy-done.4
  123.9 1.3 convolution_add_fusion.1
  125.2 0.1 copy-done.3
  125.3 2.7 %fusion = bf16[2112,512]{1,0:T(8,128)(2,1)} fusion(f32[2112,512]{1,0:T(8,128)S(1)} %convolution_add_fusion.1, bf16[2112,320]{1,0:T(8,128)(2,1)S(1)} %bitcast.34, bf16[512,704]{1,0:T(8,128)(2,1)S(1)} %get-tuple-element.39), kind=kOutput, calls=%fused_computation.3 | convolution fusion | flops 694222848 | bytes 8503296 | tf_op jit(solution)/shard_map/dot_general | solution.py:455
  128.0 0.6 pad_maximum_fusion.1.refs_3_
  128.6 51.5 %reduce_all.1 = (f32[264,704]{1,0:T(8,128)}, bf16[528,512]{1,0:T(8,128)(2,1)}, f32[1,704]{1,0:T(1,128)}, f32[4,4,704]{2,1,0:T(4,128)}) custom-call(f32[8,3,88,384]{3,2,1,0:T(8,128)} %fusion.15.refs_0_, f32[8,3,88,320]{3,2,1,0:T(8,128)} %fusion.17.refs_1_, bf16[4,528,512]{2,1,0:T(8,128)(2,1)} %bitcast.32, f32[4,704]{1,0:T(4,128)} %pad_maximum_fusion.1.refs_3_), custom_call_target="tpu_custom_call" | custom-call | tf_op jit(solution)/shard_map/reduce_all/pallas_call | solution.py:358
  180.1 0.9 slice_reduce_fusion
  181.0 0.7 squeeze.7
  181.7 0.8 copy.14
  182.5 0.7 slice.79
  183.3 1.3 reduce.3
  184.5 1.9 %copy.20 = bf16[512,528]{0,1:T(8,128)(2,1)} copy(bf16[512,528]{0,1:T(8,128)(2,1)} %bitcast.39) | data formatting | bytes 1081344
  186.4 0.9 copy.21
  (15 shorter events, 0.0 us)
Async XLA Ops:
  98.8 7.3 %copy-start.2 = (bf16[512,704]{1,0:T(8,128)(2,1)S(1)}, bf16[512,704]{1,0:T(8,128)(2,1)}, u32[]{:S(2)}) copy-start(bf16[512,704]{1,0:T(8,128)(2,1)} %get-tuple-element.18) | copy-start | bytes 2162692
  98.8 7.3 %copy-start.7 = (bf16[512,704]{1,0:T(8,128)(2,1)S(1)}, bf16[512,704]{1,0:T(8,128)(2,1)}, u32[]{:S(2)}) copy-start(bf16[512,704]{1,0:T(8,128)(2,1)} %get-tuple-element.19) | copy-start | bytes 2162692
  99.7 5.2 %collective-permute-start = (bf16[2,704]{1,0:T(2,128)(2,1)S(1)}, bf16[2,704]{1,0:T(2,128)(2,1)S(1)}, u32[]{:S(2)}, u32[]{:S(2)}) collective-permute-start(bf16[2,704]{1,0:T(2,128)(2,1)S(1)} %slice.64), channel_id=1, source_target_pairs={{0,4},{4,8},{8,12},{12,16},{16,20},{20,24},{24,28},{1,5},{5,9},{9,... | collective-permute-start | bytes 8456 | tf_op jit(solution)/shard_map/ppermute | solution.py:21
  113.4 1.6 copy-start
  118.0 3.0 %copy-start.1 = (bf16[8,264,384]{2,1,0:T(8,128)(2,1)S(1)}, bf16[8,264,384]{2,1,0:T(8,128)(2,1)}, u32[]{:S(2)}) copy-start(bf16[8,264,384]{2,1,0:T(8,128)(2,1)} %get-tuple-element.21) | copy-start | bytes 4866052
  121.1 1.4 copy-start.5
  122.5 1.4 copy-start.4
  123.9 1.4 copy-start.3
  180.1 6.3 %copy-start.6 = (f32[264,704]{1,0:T(8,128)S(1)}, f32[264,704]{1,0:T(8,128)}, u32[]{:S(2)}) copy-start(f32[264,704]{1,0:T(8,128)} %get-tuple-element.46) | copy-start | bytes 2230276
